TPU v7x, 512 devices: a whole 4x8x8 slice. The times are simulated.
512 devices in a mesh: sp: 32 (over z, x), dp: 16 (over y, core).
Axes of the slice: x: 4, y: 8, z: 8, core: 2. Of those that a mesh axis runs over, the one named last changes fastest.
Arguments:
- tokens: bfloat16 [16, 16384, 2048], P('dp', 'sp'), may hold values from -6 to 6
- segments: int32 [16, 16384], P('dp', 'sp'), may hold values from 0 to 15, never falling along the last dimension, each value on 1 to 2048 neighbouring positions
- w_lin: bfloat16 [2048, 1024], P('dp'), may hold values from -0.125 to 0.125
- w_gate: bfloat16 [2048, 1024], P('dp'), may hold values from -0.125 to 0.125
- w_out: bfloat16 [1024, 2048], P(None, 'dp'), may hold values from -0.1875 to 0.1875
- conv_kernel: float32 [31, 1024], replicated, may hold values from -1 to 1
- conv_bias: float32 [1024], replicated, may hold values from -3 to 3
- norm_gain: float32 [1024], replicated, may hold values from 0.1 to 1.9
- norm_bias: float32 [1024], replicated, may hold values from -3 to 3
Outputs:
- mixed_out: bfloat16 [16, 16384, 2048], P('dp', 'sp')
Inputs may be any that keep to these rules, and one draw needn't show every extreme that they name: `segments`: within each sequence document numbers never fall; a document is a run of equal numbers of at most four times 512 positions.
All inputs are finite; a program needn't handle non-finite values.
Results may differ from a plain program's by a relative error of at most 0.0062.
Values may be sent and summed in bfloat16 or wider, within the bound.
A program may use at most 64 MiB of HBM per device.

v0:
```python
import jax
import jax.numpy as jnp
from jax import lax
from jax.sharding import PartitionSpec as P

K = 31


def sent_together(arrays, axis, dim, along):
    both = jnp.concatenate(arrays, axis=along)
    result, at, outs = (lax.all_gather(both, axis, axis=dim, tiled=True), 0, [])
    for a in arrays:
        outs.append(lax.slice_in_dim(result, at, at + a.shape[along], axis=along))
        at += a.shape[along]
    return tuple(outs)


def from_behind(value, axis, by):
    devices = lax.axis_size(axis)
    pairs = [(i, i + by) for i in range(devices) if 0 <= i + by < devices]
    return lax.ppermute(value, axis, pairs)


def conv_doc(values, doc_ids, kernel, bias):
    taps = kernel.shape[0]
    reach = taps - 1
    length = values.shape[1]
    place = lax.iota(jnp.int32, length)
    change = jnp.concatenate([jnp.ones((1,), jnp.bool_), doc_ids[1:] != doc_ids[:-1]])
    begins = lax.cummax(jnp.where(change, place, 0), axis=0)[reach:]
    here = place[reach:]
    total = bias[:, None] + kernel[reach][:, None] * values[:, reach:].astype(jnp.float32)
    for back in range(1, taps):
        piece = values[:, reach - back : length - back].astype(jnp.float32)
        keep = here - back >= begins
        total = total + kernel[reach - back][:, None] * jnp.where(keep[None, :], piece, 0.0)
    return total


def body(tokens, segments, w_lin, w_gate, w_out, conv_kernel, conv_bias, norm_gain, norm_bias):
    rows = tokens[0]
    doc_ids = segments[0]
    count = rows.shape[0]
    reach = K - 1
    pieces = sent_together((w_lin, w_gate), "dp", 0, 1)
    first = jnp.einsum("rc,tr->ct", pieces[0], rows, preferred_element_type=jnp.float32)
    second = jnp.einsum("rc,tr->ct", pieces[1], rows, preferred_element_type=jnp.float32)
    glu = (first * jax.nn.sigmoid(second)).astype(jnp.bfloat16)
    tail, tail_ids = from_behind((glu[:, count - reach :], doc_ids[count - reach :]), "sp", 1)
    extended = jnp.concatenate([tail, glu], axis=1)
    ext_ids = jnp.concatenate([tail_ids, doc_ids], axis=0)
    conv = conv_doc(extended, ext_ids, conv_kernel, conv_bias)
    conved = lax.optimization_barrier(conv.astype(jnp.bfloat16))
    values = conved.astype(jnp.float32)
    mean = jnp.mean(values, axis=0, keepdims=True)
    var = jnp.mean(jnp.square(values - mean), axis=0, keepdims=True)
    normed = (values - mean) * lax.rsqrt(var + 1e-05) * norm_gain[:, None] + norm_bias[:, None]
    act = jax.nn.silu(normed).astype(jnp.bfloat16)
    mixed_out = jnp.einsum(
        "ct,cr->tr",
        act,
        lax.all_gather(w_out, "dp", axis=1, tiled=True),
        preferred_element_type=jnp.float32,
    ).astype(jnp.bfloat16)
    return mixed_out[None]


def solution(mesh):
    placed = (
        P("dp", "sp", None),
        P("dp", "sp"),
        P("dp", None),
        P("dp", None),
        P(None, "dp"),
        P(),
        P(),
        P(),
        P(),
    )
    return jax.shard_map(
        body, mesh=mesh, in_specs=placed, out_specs=P("dp", "sp", None), check_vma=False
    )
```

profile of v0, /device:TPU:1, one launch (start us, length us, event | category | flops | bytes accessed | tf_op | source)
XLA Modules:
  0.0 140.4 jit_solution(699867994584362061)
XLA Ops:
  6.5 0.0 copy-start
  6.5 0.0 copy-start.2
  6.5 0.0 all-gather.3.cloned.1.call-start
  6.5 2.0 %pad_maximum_fusion.1 = bf16[128,2048]{1,0:T(8,128)(2,1)} fusion(bf16[128,1024]{1,0:T(8,128)(2,1)} %param.12, bf16[128,1024]{1,0:T(8,128)(2,1)} %param.11), kind=kLoop, calls=%fused_computation.92 | loop fusion | flops 1048576 | bytes 1048576 | tf_op jit(solution)/shard_map/concatenate | solution.py:10
  8.6 0.0 all-gather.3.cloned.1.call-update
  8.6 0.0 all-gather.5.cloned.1.call-start
  8.6 0.7 all-gather.5.cloned.1.call-update
  9.3 0.7 slice_bitcast_fusion
  10.1 3.9 %collective-permute-start = (s32[30]{0:T(128)S(1)}, s32[30]{0:T(128)S(1)}, u32[]{:S(2)}, u32[]{:S(2)}) collective-permute-start(s32[30]{0:T(128)S(1)} %slice_bitcast_fusion), channel_id=1, source_target_pairs={{0,16},{16,32},{32,48},{48,64},{64,80},{80,96},{96,112},{112,128},... | collective-permute-start | bytes 368 | tf_op jit(solution)/shard_map/ppermute | solution.py:21
  14.0 1.4 fusion.58
  15.4 1.1 fusion.59
  16.5 0.0 collective-permute-done
  16.5 0.0 copy-done.2
  16.5 0.1 pad_add_fusion
  16.6 0.1 slice_compare_fusion
  16.7 0.1 iota_select_fusion
  16.8 0.3 reduce-window.9
  17.0 0.1 slice.286
  17.1 0.1 slice_reduce_fusion
  17.3 0.1 maximum_bitcast_fusion
  17.3 0.1 add_compare_fusion.29
  17.4 0.1 add_compare_fusion.20
  17.5 0.1 add_compare_fusion.11
  17.6 55.9 %all-gather.3.cloned.1.call-done = bf16[2048,2048]{1,0:T(8,128)(2,1)} async-done(((bf16[128,2048]{1,0:T(8,128)(2,1)}), bf16[2048,2048]{1,0:T(8,128)(2,1)}) %all-gather.3.cloned.1.call-update) | async-done | bytes 8388624 | tf_op jit(solution)/shard_map/all_gather | solution.py:11
  73.5 0.0 copy-done
  73.5 0.0 copy-start.3
  73.5 4.7 %fusion = f32[1024,512]{0,1:T(8,128)S(1)} fusion(bf16[2048,2048]{1,0:T(8,128)(2,1)} %all-gather.3.cloned.1.call-done, bf16[1,512,2048]{2,1,0:T(8,128)(2,1)S(1)} %copy-done), kind=kOutput, calls=%fused_computation.29 | convolution fusion | flops 2147483648 | bytes 8388608 | tf_op jit(solution)/shard_map/rc,tr->ct/dot_general | solution.py:47
  78.2 0.0 copy-done.3
  78.2 0.0 copy-start.1
  78.2 2.5 %multiply_convert_fusion = bf16[1024,512]{0,1:T(8,128)(2,1)S(1)} fusion(f32[1024,512]{0,1:T(8,128)S(1)} %fusion, bf16[2048,2048]{1,0:T(8,128)(2,1)S(1)} %copy-done.3, bf16[1,512,2048]{2,1,0:T(8,128)(2,1)S(1)} %copy-done), kind=kOutput, calls=%fused_computation.51 | convolution fusion | flops 2150105088 | bytes 9437184 | tf_op jit(solution)/shard_map/rc,tr->ct/dot_general | solution.py:46
  80.7 3.1 %collective-permute-start.1 = (bf16[1024,30]{0,1:T(8,128)(2,1)S(1)}, bf16[1024,30]{0,1:T(8,128)(2,1)S(1)}, u32[]{:S(2)}, u32[]{:S(2)}) collective-permute-start(bf16[1024,30]{0,1:T(8,128)(2,1)S(1)} %slice.351), channel_id=1, source_target_pairs={{0,16},{16,32},{32,48},{48,64},{64,80},{80,96},{96,112},{112,128},... | collective-permute-start | bytes 184328 | tf_op jit(solution)/shard_map/ppermute | solution.py:21
  83.8 0.1 add_compare_fusion.2
  83.9 1.2 collective-permute-done.1
  85.2 0.0 copy-done.1
  85.2 0.0 copy-start.4
  85.2 0.0 copy-start.5
  85.2 15.9 %add_convert_fusion = bf16[1024,512]{0,1:T(8,128)(2,1)S(1)} fusion(bf16[1024,512]{0,1:T(8,128)(2,1)S(1)} %multiply_convert_fusion, bf16[1024,30]{0,1:T(8,128)(2,1)S(1)} %collective-permute-done.1, f32[1024]{0:T(1024)S(1)} %bitcast.77, f32[1024]{0:T(1024)S(1)} %bitcast.78, f32[1024]{0:T(1024)S(1)} %bitcast.49, f32[1024]{0:T(1024)S(1)} %bitcast.50, ...), kind=kLoop, calls=%fused_computation.50 | loop fusion | flops 112197632 | bytes 2305024 | tf_op jit(solution)/shard_map/convert_element_type | solution.py:53
  101.0 0.2 convert_reduce_fusion
  101.3 0.4 fusion.7
  101.7 25.5 %all-gather.5.cloned.1.call-done = bf16[1024,2048]{1,0:T(8,128)(2,1)} async-done(((bf16[1024,128]{1,0:T(8,128)(2,1)}), bf16[1024,2048]{1,0:T(8,128)(2,1)}) %all-gather.5.cloned.1.call-update) | async-done | bytes 4194320 | tf_op jit(solution)/shard_map/all_gather | solution.py:62
  127.2 0.0 copy-done.4
  127.2 0.0 copy-done.5
  127.2 6.4 %fusion.4 = bf16[1,512,2048]{2,1,0:T(8,128)(2,1)} fusion(bf16[1024,2048]{1,0:T(8,128)(2,1)} %all-gather.5.cloned.1.call-done, bf16[1024,512]{0,1:T(8,128)(2,1)S(1)} %add_convert_fusion, f32[1024]{0:T(1024)S(1)} %copy-done.4, f32[1024]{0:T(1024)S(1)} %copy-done.5, f32[512]{0:T(512)S(1)} %add_rsqrt_fusion, f32[512]{0:T(512)S(1)} %broadcast_multiply_fusion), kind=kOutput, calls=%fused_computation.34 | convolution fusion | flops 2153775104 | bytes 7352320 | tf_op jit(solution)/shard_map/ct,cr->tr/dot_general | solution.py:59
  (6 shorter events, 0.1 us)
Async XLA Ops:
  6.5 67.0 %copy-start = (bf16[1,512,2048]{2,1,0:T(8,128)(2,1)S(1)}, bf16[1,512,2048]{2,1,0:T(8,128)(2,1)}, u32[]{:S(2)}) copy-start(bf16[1,512,2048]{2,1,0:T(8,128)(2,1)} %param.9) | copy-start | bytes 6291460
  6.5 10.0 %copy-start.2 = (s32[1,512]{1,0:T(1,128)S(1)}, s32[1,512]{1,0:T(1,128)}, u32[]{:S(2)}) copy-start(s32[1,512]{1,0:T(1,128)} %param.10) | copy-start | bytes 6148
  6.5 67.0 %all-gather.3.cloned.1.call-start = ((), (), s32[]{:S(2)}) async-start(), calls=%async_computation | async-start | bytes 8912896 | tf_op jit(solution)/shard_map/all_gather | solution.py:11
  8.6 118.6 %all-gather.5.cloned.1.call-start = ((), (), s32[]{:S(2)}) async-start(), calls=%async_computation.1 | async-start | bytes 4456448 | tf_op jit(solution)/shard_map/all_gather | solution.py:62
  10.1 6.4 %collective-permute-start = (s32[30]{0:T(128)S(1)}, s32[30]{0:T(128)S(1)}, u32[]{:S(2)}, u32[]{:S(2)}) collective-permute-start(s32[30]{0:T(128)S(1)} %slice_bitcast_fusion), channel_id=1, source_target_pairs={{0,16},{16,32},{32,48},{48,64},{64,80},{80,96},{96,112},{112,128},... | collective-permute-start | bytes 368 | tf_op jit(solution)/shard_map/ppermute | solution.py:21
  73.5 4.7 %copy-start.3 = (bf16[2048,2048]{1,0:T(8,128)(2,1)S(1)}, bf16[2048,2048]{1,0:T(8,128)(2,1)}, u32[]{:S(2)}) copy-start(bf16[2048,2048]{1,0:T(8,128)(2,1)} %all-gather.3.cloned.1.call-done) | copy-start | bytes 25165828
  78.2 7.0 %copy-start.1 = (f32[1024]{0:T(1024)S(1)}, f32[1024]{0:T(1024)}, u32[]{:S(2)}) copy-start(f32[1024]{0:T(1024)} %param.15) | copy-start | bytes 12292
  80.7 4.4 %collective-permute-start.1 = (bf16[1024,30]{0,1:T(8,128)(2,1)S(1)}, bf16[1024,30]{0,1:T(8,128)(2,1)S(1)}, u32[]{:S(2)}, u32[]{:S(2)}) collective-permute-start(bf16[1024,30]{0,1:T(8,128)(2,1)S(1)} %slice.351), channel_id=1, source_target_pairs={{0,16},{16,32},{32,48},{48,64},{64,80},{80,96},{96,112},{112,128},... | collective-permute-start | bytes 184328 | tf_op jit(solution)/shard_map/ppermute | solution.py:21
  85.2 42.0 %copy-start.4 = (f32[1024]{0:T(1024)S(1)}, f32[1024]{0:T(1024)}, u32[]{:S(2)}) copy-start(f32[1024]{0:T(1024)} %param.17) | copy-start | bytes 12292
  85.2 42.0 %copy-start.5 = (f32[1024]{0:T(1024)S(1)}, f32[1024]{0:T(1024)}, u32[]{:S(2)}) copy-start(f32[1024]{0:T(1024)} %param.16) | copy-start | bytes 12292
Sparse Core Ops, SparseCore 0:
  9.5 64.0 all-gather.2
  75.6 51.5 all-gather.4
where the time goes:
time: 141 us; the launch traced here: 140 us
  waiting for transfers between devices  83.4 us (59%)
  other arithmetic  19.5 us (14%)
  matrix products  13.5 us (10%)
  between operations  13.5 us (10%)
  starting transfers between devices  7.06 us (5%)
  local copies, waits for them, and re-layouts  3.47 us (2%)
    all_gather x1, waiting for transfers between devices, sent_together(): result, at, outs = (lax.all_gather(both, axis, axis=dim, tiled=True), 0, [])  55.9 us
    all_gather x1, waiting for transfers between devices, body(): lax.all_gather(w_out, 'dp', axis=1, tiled=True)  25.5 us
    convert_element_type x1, other arithmetic, body(): conved = lax.optimization_barrier(conv.astype(jnp.bfloat16))  15.9 us
    ppermute x2, starting transfers between devices, from_behind(): return lax.ppermute(value, axis, pairs)  7.01 us
    dot_general x1, matrix products, body(): jnp.einsum('ct,cr->tr', act, lax.all_gather(w_out, 'dp', axis=1, tiled=Tr...  6.35 us
    dot_general x1, matrix products, body(): jnp.einsum('rc,tr->ct', pieces[1], rows, preferred_element_type=jnp.float32)  4.66 us
  transfers between devices with their start and end apart: 4, of which 3 were waited for; matrix products, arithmetic and copies ran while one was open for 20% of the time, Pallas kernels for 0%

commit v1 on v0

--- a/solution.py
+++ b/solution.py
@@ -4,6 +4,11 @@
 from jax.sharding import PartitionSpec as P
 
 K = 31
+
+
+def gather_from_all(array, axis, dim):
+    copies = jnp.concatenate([array] * lax.axis_size(axis), axis=dim)
+    return lax.all_to_all(copies, axis, dim, dim, tiled=True)
 
 
 def sent_together(arrays, axis, dim, along):
@@ -57,10 +62,7 @@
     normed = (values - mean) * lax.rsqrt(var + 1e-05) * norm_gain[:, None] + norm_bias[:, None]
     act = jax.nn.silu(normed).astype(jnp.bfloat16)
     mixed_out = jnp.einsum(
-        "ct,cr->tr",
-        act,
-        lax.all_gather(w_out, "dp", axis=1, tiled=True),
-        preferred_element_type=jnp.float32,
+        "ct,cr->tr", act, gather_from_all(w_out, "dp", 1), preferred_element_type=jnp.float32
     ).astype(jnp.bfloat16)
     return mixed_out[None]
 

time: 141 us -> 207 us (1.47)
  waiting for transfers between devices: 83.4 us -> 131 us
  local copies, waits for them, and re-layouts: 3.47 us -> 16.5 us
  starting transfers between devices: 7.06 us -> 14.6 us
  matrix products: 13.5 us -> 11.3 us
    all_gather x1, waiting for transfers between devices: 55.9 us -> 131 us  [sent_together(): result, at, outs = (lax.all_gather(both, axis, axis=dim, tiled=True), 0, [])]
    all_gather x1 -> x0, waiting for transfers between devices: 25.5 us -> none  [body(): lax.all_gather(w_out, 'dp', axis=1, tiled=True)]
    all_to_all x0 -> x2, local copies, waits for them, and re-layouts: none -> 12.7 us  [gather_from_all(): return lax.all_to_all(copies, axis, dim, dim, tiled=True)]
    all_to_all x0 -> x1, starting transfers between devices: none -> 11.3 us  [gather_from_all(): return lax.all_to_all(copies, axis, dim, dim, tiled=True)]
    ppermute x2, starting transfers between devices: 7.01 us -> 3.34 us  [from_behind(): return lax.ppermute(value, axis, pairs)]
    unnamed x12 -> x34, local copies, waits for them, and re-layouts: 0.03 us -> 3.37 us
    dot_general x1, matrix products: 6.35 us -> 4.2 us  [body(): jnp.einsum('ct,cr->tr', act, gather_from_all(w_out, 'dp', 1), preferred_e...]
  transfers between devices with their start and end apart: 4 -> 4, of which waited for: 3 -> 2; matrix products, arithmetic and copies ran while one was open for 20% -> 11% of each run, Pallas kernels for 0% -> 0%
where the time goes in v1:
time: 207 us
  waiting for transfers between devices  131 us (63%)
  other arithmetic  19.7 us (10%)
  local copies, waits for them, and re-layouts  16.5 us (8%)
  starting transfers between devices  14.6 us (7%)
  between operations  13.7 us (7%)
  matrix products  11.3 us (5%)
    all_gather x1, waiting for transfers between devices, sent_together(): result, at, outs = (lax.all_gather(both, axis, axis=dim, tiled=True), 0, [])  131 us
    convert_element_type x1, other arithmetic, body(): conved = lax.optimization_barrier(conv.astype(jnp.bfloat16))  16.1 us
    all_to_all x2, local copies, waits for them, and re-layouts, gather_from_all(): return lax.all_to_all(copies, axis, dim, dim, tiled=True)  12.7 us
    all_to_all x1, starting transfers between devices, gather_from_all(): return lax.all_to_all(copies, axis, dim, dim, tiled=True)  11.3 us
    dot_general x1, matrix products, body(): jnp.einsum('rc,tr->ct', pieces[1], rows, preferred_element_type=jnp.float32)  4.66 us
    dot_general x1, matrix products, body(): jnp.einsum('ct,cr->tr', act, gather_from_all(w_out, 'dp', 1), preferred_e...  4.2 us
  transfers between devices with their start and end apart: 4, of which 2 were waited for; matrix products, arithmetic and copies ran while one was open for 11% of the time, Pallas kernels for 0%

profile of v1, /device:TPU:1, one launch (start us, length us, event | category | flops | bytes accessed | tf_op | source)
XLA Modules:
  0.0 206.9 jit_solution(9880313048619763233)
XLA Ops:
  6.5 0.0 copy-start
  6.5 0.0 all-gather.2.cloned.1.call-start
  6.5 2.0 pad_maximum_fusion.1
  8.6 0.0 all-gather.2.cloned.1.call-update
  8.6 1.1 copy.10
  10.1 0.0 copy-start.1
  10.1 2.0 copy-done.1
  12.1 6.3 %copy.26 = bf16[1024,16,128]{2,0,1:T(8,128)(2,1)} copy(bf16[1024,16,128]{0,2,1:T(8,128)(2,1)} %bitcast.50) | data formatting | bytes 8388608 | tf_op jit(solution)/shard_map/all_to_all | solution.py:11
  18.4 0.0 copy-start.5
  18.4 0.0 copy-start.3
  18.4 11.3 %all-to-all-start = ((bf16[1024,16,128]{2,0,1:T(8,128)(2,1)}), bf16[1024,16,128]{2,0,1:T(8,128)(2,1)}, u32[]{:S(2)}, u32[]{:S(2)}) async-start(bf16[1024,16,128]{2,0,1:T(8,128)(2,1)} %copy.26), calls=%async_computation | async-start | bytes 8388608 | tf_op jit(solution)/shard_map/all_to_all | solution.py:11
  29.7 0.0 copy-done.5
  29.7 0.1 slice_bitcast_fusion
  29.8 1.3 collective-permute-start
  31.0 0.0 copy-done.3
  31.0 0.1 fusion.58
  31.2 0.6 collective-permute-done
  31.7 0.1 pad_add_fusion
  31.8 0.1 slice_compare_fusion
  31.9 0.1 iota_select_fusion
  32.0 0.3 reduce-window.9
  32.3 0.1 slice.286
  32.4 0.1 slice_reduce_fusion
  32.5 0.1 maximum_bitcast_fusion
  32.6 0.1 add_compare_fusion.20
  32.6 0.1 add_compare_fusion.11
  32.7 0.1 add_compare_fusion.29
  32.8 130.6 %all-gather.2.cloned.1.call-done = bf16[2048,2048]{1,0:T(8,128)(2,1)} async-done(((bf16[128,2048]{1,0:T(8,128)(2,1)}), bf16[2048,2048]{1,0:T(8,128)(2,1)}) %all-gather.2.cloned.1.call-update) | async-done | bytes 8388624 | tf_op jit(solution)/shard_map/all_gather | solution.py:16
  163.4 0.0 copy-done
  163.4 0.0 copy-start.6
  163.4 4.7 %fusion = f32[1024,512]{0,1:T(8,128)S(1)} fusion(bf16[2048,2048]{1,0:T(8,128)(2,1)} %all-gather.2.cloned.1.call-done, bf16[1,512,2048]{2,1,0:T(8,128)(2,1)S(1)} %copy-done), kind=kOutput, calls=%fused_computation.29 | convolution fusion | flops 2147483648 | bytes 8388608 | tf_op jit(solution)/shard_map/rc,tr->ct/dot_general | solution.py:52
  168.1 0.0 copy-done.6
  168.1 2.4 %multiply_convert_fusion = bf16[1024,512]{0,1:T(8,128)(2,1)S(1)} fusion(f32[1024,512]{0,1:T(8,128)S(1)} %fusion, bf16[2048,2048]{1,0:T(8,128)(2,1)S(1)} %copy-done.6, bf16[1,512,2048]{2,1,0:T(8,128)(2,1)S(1)} %copy-done), kind=kOutput, calls=%fused_computation.51 | convolution fusion | flops 2150105088 | bytes 9437184 | tf_op jit(solution)/shard_map/rc,tr->ct/dot_general | solution.py:51
  170.5 2.1 collective-permute-start.1
  172.6 0.1 add_compare_fusion.2
  172.7 0.0 all-to-all-done
  172.7 6.4 %copy.27 = bf16[1024,16,128]{0,2,1:T(8,128)(2,1)} copy(bf16[1024,16,128]{2,0,1:T(8,128)(2,1)} %all-to-all-done) | data formatting | bytes 8388608 | tf_op jit(solution)/shard_map/all_to_all | solution.py:11
  179.1 0.0 collective-permute-done.1
  179.1 0.0 copy-done.4
  179.1 0.0 copy-start.7
  179.1 0.0 copy-start.8
  179.1 16.1 %add_convert_fusion = bf16[1024,512]{0,1:T(8,128)(2,1)S(1)} fusion(bf16[1024,512]{0,1:T(8,128)(2,1)S(1)} %multiply_convert_fusion, bf16[1024,30]{0,1:T(8,128)(2,1)S(1)} %collective-permute-done.1, f32[1024]{0:T(1024)S(1)} %bitcast.81, f32[1024]{0:T(1024)S(1)} %bitcast.82, f32[1024]{0:T(1024)S(1)} %bitcast.53, f32[1024]{0:T(1024)S(1)} %bitcast.54, ...), kind=kLoop, calls=%fused_computation.50 | loop fusion | flops 112197632 | bytes 2305024 | tf_op jit(solution)/shard_map/convert_element_type | solution.py:58
  195.2 0.2 convert_reduce_fusion
  195.4 0.4 fusion.7
  195.9 0.0 copy-done.2
  195.9 0.0 copy-done.7
  195.9 0.0 copy-done.8
  195.9 4.2 %fusion.4 = bf16[1,512,2048]{2,1,0:T(8,128)(2,1)} fusion(bf16[1024,2048]{0,1:T(8,128)(2,1)S(1)} %bitcast.51, bf16[1024,512]{0,1:T(8,128)(2,1)S(1)} %add_convert_fusion, f32[1024]{0:T(1024)S(1)} %copy-done.7, f32[1024]{0:T(1024)S(1)} %copy-done.8, f32[512]{0:T(512)S(1)} %add_rsqrt_fusion, f32[512]{0:T(512)S(1)} %broadcast_multiply_fusion), kind=kOutput, calls=%fused_computation.34 | convolution fusion | flops 2153775104 | bytes 7352320 | tf_op jit(solution)/shard_map/ct,cr->tr/dot_general | solution.py:64
  (25 shorter events, 0.4 us)
Async XLA Ops:
  6.5 156.9 %copy-start = (bf16[1,512,2048]{2,1,0:T(8,128)(2,1)S(1)}, bf16[1,512,2048]{2,1,0:T(8,128)(2,1)}, u32[]{:S(2)}) copy-start(bf16[1,512,2048]{2,1,0:T(8,128)(2,1)} %param.9) | copy-start | bytes 6291460
  6.5 156.9 %all-gather.2.cloned.1.call-start = ((), (), s32[]{:S(2)}) async-start(), calls=%async_computation.1 | async-start | bytes 8912896 | tf_op jit(solution)/shard_map/all_gather | solution.py:16
  10.1 2.0 copy-start.1
  18.4 11.3 %copy-start.5 = (s32[1,512]{1,0:T(1,128)S(1)}, s32[1,512]{1,0:T(1,128)}, u32[]{:S(2)}) copy-start(s32[1,512]{1,0:T(1,128)} %param.10) | copy-start | bytes 6148
  18.4 12.6 %copy-start.3 = (f32[31,1024]{1,0:T(8,128)S(1)}, f32[31,1024]{1,0:T(8,128)}, u32[]{:S(2)}) copy-start(f32[31,1024]{1,0:T(8,128)} %param.14) | copy-start | bytes 380932
  18.4 154.3 %all-to-all-start = ((bf16[1024,16,128]{2,0,1:T(8,128)(2,1)}), bf16[1024,16,128]{2,0,1:T(8,128)(2,1)}, u32[]{:S(2)}, u32[]{:S(2)}) async-start(bf16[1024,16,128]{2,0,1:T(8,128)(2,1)} %copy.26), calls=%async_computation | async-start | bytes 8388608 | tf_op jit(solution)/shard_map/all_to_all | solution.py:11
  29.8 2.0 collective-permute-start
  163.4 4.7 %copy-start.6 = (bf16[2048,2048]{1,0:T(8,128)(2,1)S(1)}, bf16[2048,2048]{1,0:T(8,128)(2,1)}, u32[]{:S(2)}) copy-start(bf16[2048,2048]{1,0:T(8,128)(2,1)} %all-gather.2.cloned.1.call-done) | copy-start | bytes 25165828
  170.5 8.6 %collective-permute-start.1 = (bf16[1024,30]{0,1:T(8,128)(2,1)S(1)}, bf16[1024,30]{0,1:T(8,128)(2,1)S(1)}, u32[]{:S(2)}, u32[]{:S(2)}) collective-permute-start(bf16[1024,30]{0,1:T(8,128)(2,1)S(1)} %slice.351), channel_id=1, source_target_pairs={{0,16},{16,32},{32,48},{48,64},{64,80},{80,96},{96,112},{112,128},... | collective-permute-start | bytes 184328 | tf_op jit(solution)/shard_map/ppermute | solution.py:26
  172.7 6.4 %copy-start.4 = (f32[1024]{0:T(1024)S(1)}, f32[1024]{0:T(1024)}, u32[]{:S(2)}) copy-start(f32[1024]{0:T(1024)} %param.15) | copy-start | bytes 12292
  179.1 16.8 %copy-start.2 = (bf16[1024,16,128]{0,2,1:T(8,128)(2,1)S(1)}, bf16[1024,16,128]{0,2,1:T(8,128)(2,1)}, u32[]{:S(2)}) copy-start(bf16[1024,16,128]{0,2,1:T(8,128)(2,1)} %copy.27) | copy-start | bytes 12582916
  179.1 16.8 %copy-start.7 = (f32[1024]{0:T(1024)S(1)}, f32[1024]{0:T(1024)}, u32[]{:S(2)}) copy-start(f32[1024]{0:T(1024)} %param.17) | copy-start | bytes 12292
  179.1 16.8 %copy-start.8 = (f32[1024]{0:T(1024)S(1)}, f32[1024]{0:T(1024)}, u32[]{:S(2)}) copy-start(f32[1024]{0:T(1024)} %param.16) | copy-start | bytes 12292
Sparse Core Ops, SparseCore 0:
  9.5 153.9 all-gather.1
